TPU v7x, 32 devices: a whole 2x2x4 slice. The times are simulated.
32 devices in a mesh: fs: 8 (over z, y), tp: 4 (over x, core).
Axes of the slice: x: 2, y: 2, z: 4, core: 2. Of those that a mesh axis runs over, the one named last changes fastest.
Arguments:
- tokens: bfloat16 [6144, 2048], P(('fs', 'tp')), may hold values from -60 to 60
- norm_gain: float32 [2048], P('fs'), may hold values from 0.1 to 1.9
- gate_weight: float32 [2048, 5632], P('fs', 'tp'), may hold values from -0.125 to 0.125
- up_weight: float32 [2048, 5632], P('fs', 'tp'), may hold values from -0.125 to 0.125
- down_weight: float32 [2048, 5632], P('fs', 'tp'), may hold values from -0.078125 to 0.078125
Outputs:
- mixed_rows: bfloat16 [6144, 2048], P(('fs', 'tp'))
- gate_out: bfloat16 [2048, 5632], P(None, 'tp')
- up_out: bfloat16 [2048, 5632], P(None, 'tp')
- down_out: bfloat16 [2048, 5632], P(None, 'tp')
All inputs are finite; a program needn't handle non-finite values.
Results may differ from a plain program's by a relative error of at most 0.014.
Values may be sent and summed in bfloat16 or wider, within the bound.
A program may use at most 128 MiB of HBM per device.

v0:
```python
import jax
import jax.numpy as jnp
from jax import lax
from jax.sharding import PartitionSpec as P


def normalize(source):
    widened = source.astype(jnp.float32)
    return (widened * lax.rsqrt(jnp.mean(widened * widened, axis=1, keepdims=True) + 1e-06)).astype(
        jnp.bfloat16
    )


def shards(tokens, norm_gain, gate_weight, up_weight, down_weight):
    row_gain = norm_gain[:, None]
    gate_local = (gate_weight * row_gain).astype(jnp.bfloat16)
    up_local = (up_weight * row_gain).astype(jnp.bfloat16)
    down_local = down_weight.astype(jnp.bfloat16)
    normed = normalize(tokens)
    gathered = lax.all_gather(normed, "tp", axis=0, tiled=True)
    down_whole = lax.all_gather(down_local, "fs", axis=0, tiled=True)
    gate_piece = lax.all_gather(gate_local, "fs", axis=0, tiled=True)
    up_piece = lax.all_gather(up_local, "fs", axis=0, tiled=True)
    gate_acc = jnp.dot(gathered, gate_piece, preferred_element_type=jnp.float32)
    up_acc = jnp.dot(gathered, up_piece, preferred_element_type=jnp.float32)
    hidden = (jax.nn.silu(gate_acc) * up_acc).astype(jnp.bfloat16)
    partial_value = lax.dot_general(
        hidden, down_whole, (((1,), (1,)), ((), ())), preferred_element_type=jnp.float32
    )
    mixed_rows = lax.psum_scatter(
        lax.optimization_barrier(partial_value.astype(jnp.bfloat16))
        .astype(jnp.float32)
        .astype(jnp.bfloat16),
        "tp",
        scatter_dimension=0,
        tiled=True,
    )
    return (mixed_rows, gate_piece, up_piece, down_whole)


def solution(mesh):
    in_specs = (P(("fs", "tp"), None), P("fs"), P("fs", "tp"), P("fs", "tp"), P("fs", "tp"))
    out_specs = (P(("fs", "tp"), None), P(None, "tp"), P(None, "tp"), P(None, "tp"))
    return jax.shard_map(shards, mesh=mesh, in_specs=in_specs, out_specs=out_specs, check_vma=False)
```

profile of v0, /device:TPU:0, one launch (start us, length us, event | category | flops | bytes accessed | tf_op | source)
XLA Modules:
  0.0 397.9 jit_solution(9030108663980922372)
XLA Ops:
  7.2 0.0 all-gather.5.cloned.1.call-start
  7.2 1.5 fusion
  8.7 2.2 fusion.1
  10.9 0.0 all-gather.5.cloned.1.call-update
  10.9 0.0 all-gather.7.cloned.1.call-start
  11.0 3.2 multiply_convert_fusion.1
  14.2 0.0 all-gather.7.cloned.1.call-update
  14.2 0.0 all-gather.11.cloned.1.call-start
  14.2 0.9 convert_element_type.28
  15.2 0.0 all-gather.11.cloned.1.call-update
  15.2 0.0 all-gather.9.cloned.1.call-start
  15.3 0.5 all-gather.9.cloned.1.call-update
  15.8 0.0 reduce-scatter.2.cloned.1.call-start
  15.8 26.5 %all-gather.5.cloned.1.call-done = bf16[768,2048]{1,0:T(8,128)(2,1)} async-done(((bf16[192,2048]{1,0:T(8,128)(2,1)}), bf16[768,2048]{1,0:T(8,128)(2,1)}) %all-gather.5.cloned.1.call-update) | async-done | bytes 3145744 | tf_op jit(solution)/shard_map/all_gather | solution.py:20
  42.3 95.1 %all-gather.7.cloned.1.call-done = bf16[2048,1408]{1,0:T(8,128)(2,1)} async-done(((bf16[256,1408]{1,0:T(8,128)(2,1)}), bf16[2048,1408]{1,0:T(8,128)(2,1)}) %all-gather.7.cloned.1.call-update) | async-done | bytes 5767184 | tf_op jit(solution)/shard_map/all_gather | solution.py:22
  137.4 9.7 %fusion.3 = f32[768,1408]{1,0:T(8,128)} fusion(bf16[768,2048]{1,0:T(8,128)(2,1)} %all-gather.5.cloned.1.call-done, bf16[2048,1408]{1,0:T(8,128)(2,1)} %all-gather.7.cloned.1.call-done), kind=kOutput, calls=%fused_computation.10 | convolution fusion | flops 4429185024 | bytes 13238272 | tf_op jit(solution)/shard_map/dot_general | solution.py:24
  147.1 83.6 %all-gather.11.cloned.1.call-done = bf16[2048,1408]{1,0:T(8,128)(2,1)} async-done(((bf16[256,1408]{1,0:T(8,128)(2,1)}), bf16[2048,1408]{1,0:T(8,128)(2,1)}) %all-gather.11.cloned.1.call-update) | async-done | bytes 5767184 | tf_op jit(solution)/shard_map/all_gather | solution.py:21
  230.7 93.1 %all-gather.9.cloned.1.call-done = bf16[2048,1408]{1,0:T(8,128)(2,1)} async-done(((bf16[256,1408]{1,0:T(8,128)(2,1)}), bf16[2048,1408]{1,0:T(8,128)(2,1)}) %all-gather.9.cloned.1.call-update) | async-done | bytes 5767184 | tf_op jit(solution)/shard_map/all_gather | solution.py:23
  323.8 17.3 %convolution_convert_fusion = bf16[768,2048]{1,0:T(8,128)(2,1)} fusion(bf16[2048,1408]{1,0:T(8,128)(2,1)} %all-gather.11.cloned.1.call-done, f32[768,1408]{1,0:T(8,128)} %fusion.3, bf16[768,2048]{1,0:T(8,128)(2,1)S(1)} %copy-done.1, bf16[2048,1408]{1,0:T(8,128)(2,1)} %all-gather.9.cloned.1.call-done), kind=kOutput, calls=%fused_computation.1 | convolution fusion | flops 8866430976 | bytes 22151168 | tf_op jit(solution)/shard_map/dot_general | solution.py:27
  341.2 0.0 reduce-scatter.2.cloned.1.call-update
  341.2 36.2 %reduce-scatter.2.cloned.1.call-done = bf16[192,2048]{1,0:T(8,128)(2,1)} async-done(((bf16[768,2048]{1,0:T(8,128)(2,1)}), bf16[192,2048]{1,0:T(8,128)(2,1)}) %reduce-scatter.2.cloned.1.call-update) | async-done | bytes 786448 | tf_op jit(solution)/shard_map/reduce_scatter | solution.py:30
  377.4 5.7 %copy.12 = bf16[2048,1408]{1,0:T(8,128)(2,1)} copy(bf16[2048,1408]{1,0:T(8,128)(2,1)} %all-gather.7.cloned.1.call-done) | data formatting | bytes 11534336
  383.2 5.7 %copy.13 = bf16[2048,1408]{1,0:T(8,128)(2,1)} copy(bf16[2048,1408]{1,0:T(8,128)(2,1)} %all-gather.9.cloned.1.call-done) | data formatting | bytes 11534336
  388.9 2.5 copy.14
  (10 shorter events, 0.0 us)
Async XLA Ops:
  7.2 7.1 %copy-start = (f32[256,1408]{1,0:T(8,128)S(1)}, f32[256,1408]{1,0:T(8,128)}, u32[]{:S(2)}) copy-start(f32[256,1408]{1,0:T(8,128)} %param.9) | copy-start | bytes 4325380
  7.2 35.2 %all-gather.5.cloned.1.call-start = ((), (), s32[]{:S(2)}) async-start(), calls=%async_computation.1 | async-start | bytes 3932160 | tf_op jit(solution)/shard_map/all_gather | solution.py:20
  10.9 126.5 %all-gather.7.cloned.1.call-start = ((), (), s32[]{:S(2)}) async-start(), calls=%async_computation.2 | async-start | bytes 6488064 | tf_op jit(solution)/shard_map/all_gather | solution.py:22
  14.2 216.5 %all-gather.11.cloned.1.call-start = ((), (), s32[]{:S(2)}) async-start(), calls=%async_computation.4 | async-start | bytes 6488064 | tf_op jit(solution)/shard_map/all_gather | solution.py:21
  15.2 308.6 %all-gather.9.cloned.1.call-start = ((), (), s32[]{:S(2)}) async-start(), calls=%async_computation.3 | async-start | bytes 6488064 | tf_op jit(solution)/shard_map/all_gather | solution.py:23
  15.8 361.6 %reduce-scatter.2.cloned.1.call-start = ((), (), s32[]{:S(2)}) async-start(), calls=%async_computation.5 | async-start | bytes 3932160 | tf_op jit(solution)/shard_map/reduce_scatter | solution.py:30
  42.3 281.5 %copy-start.1 = (bf16[768,2048]{1,0:T(8,128)(2,1)S(1)}, bf16[768,2048]{1,0:T(8,128)(2,1)}, u32[]{:S(2)}) copy-start(bf16[768,2048]{1,0:T(8,128)(2,1)} %all-gather.5.cloned.1.call-done) | copy-start | bytes 9437188
  377.4 11.5 %slice-start = ((s8[5767168]{0:T(1024)(128)(4,1)}), s8[4194304]{0:T(1024)(128)(4,1)S(1)}, s32[]{:S(2)}) async-start(s8[5767168]{0:T(1024)(128)(4,1)} %bitcast.5), calls=%async_computation.6 | async-start | bytes 8388608
  383.2 5.7 %slice-start.1 = ((s8[5767168]{0:T(1024)(128)(4,1)}), s8[1572864]{0:T(1024)(128)(4,1)S(1)}, s32[]{:S(2)}) async-start(s8[5767168]{0:T(1024)(128)(4,1)} %bitcast.5), calls=%async_computation.7 | async-start | bytes 3145728
Sparse Core Ops, SparseCore 0:
  11.1 31.2 all-gather.4
  45.1 92.2 all-gather.6
  140.2 90.4 all-gather.10
  233.3 90.4 all-gather.8
  341.3 36.0 reduce-scatter.1
where the time goes:
time: 398 us
  waiting for transfers between devices  335 us (84%)
  matrix products  27 us (7%)
  local copies, waits for them, and re-layouts  14 us (4%)
  between operations  13.8 us (3%)
  other arithmetic  7.8 us (2%)
    all_gather x1, waiting for transfers between devices, shards(): gate_piece = lax.all_gather(gate_local, 'fs', axis=0, tiled=True)  95.1 us
    all_gather x1, waiting for transfers between devices, shards(): up_piece = lax.all_gather(up_local, 'fs', axis=0, tiled=True)  93.1 us
    all_gather x1, waiting for transfers between devices, shards(): down_whole = lax.all_gather(down_local, 'fs', axis=0, tiled=True)  83.6 us
    reduce_scatter x1, waiting for transfers between devices, shards(): lax.psum_scatter(lax.optimization_barrier(partial_value.astype(jnp.bfloat...  36.2 us
    all_gather x1, waiting for transfers between devices, shards(): gathered = lax.all_gather(normed, 'tp', axis=0, tiled=True)  26.5 us
    dot_general x1, matrix products, shards(): lax.dot_general(hidden, down_whole, (((1,), (1,)), ((), ())), preferred_e...  17.3 us
    unnamed x11, local copies, waits for them, and re-layouts  14 us
    dot_general x1, matrix products, shards(): gate_acc = jnp.dot(gathered, gate_piece, preferred_element_type=jnp.float32)  9.67 us
  transfers between devices with their start and end apart: 5, of which 5 were waited for; matrix products, arithmetic and copies ran while one was open for 3% of the time, Pallas kernels for 0%

commit v1 on v0

--- a/solution.py
+++ b/solution.py
@@ -1,7 +1,13 @@
+import functools
+
 import jax
 import jax.numpy as jnp
 from jax import lax
+from jax.experimental import pallas as pl
+from jax.experimental.pallas import tpu as pltpu
 from jax.sharding import PartitionSpec as P
+
+MESH = pl.DeviceIdType.MESH
 
 
 def normalize(source):
@@ -38,7 +44,301 @@
     return (mixed_rows, gate_piece, up_piece, down_whole)
 
 
+def kernel(
+    Z, TP, tok_ref, gain_ref, gw_ref, uw_ref, dw_ref, mix_ref, g_ref, u_ref, d_ref,
+    x_buf, sg_buf, h_buf, part_buf, in_buf,
+    zm_sem, zp_sem, y_sem, hp_sem, w_recv, x_send, x_recv, r_send, r_recv,
+):
+    fs, tp = lax.axis_index("fs"), lax.axis_index("tp")
+    z, y = fs // 2, lax.rem(fs, 2)
+    oy = 1 - y
+    pz = z + 1 - 2 * lax.rem(z, 2)
+    R, F = gw_ref.shape
+    half = R // 2
+    T = tok_ref.shape[0]
+    weights = (g_ref, u_ref, d_ref)
+
+    def dev(zz, yy):
+        return (zz * 2 + yy, tp)
+
+    def peer(p):
+        return lax.rem(tp + p, TP)
+
+    barrier = pltpu.get_barrier_semaphore()
+
+    def greet(target):
+        pl.semaphore_signal(barrier, inc=1, device_id=target, device_id_type=MESH)
+
+    greet(dev(z, oy))
+    for p in range(1, TP):
+        greet((fs, peer(p)))
+
+    @pl.when(z > 0)
+    def _():
+        greet(dev(z - 1, y))
+
+    @pl.when(z < Z - 1)
+    def _():
+        greet(dev(z + 1, y))
+
+    gain = gain_ref[...]
+    own = pl.ds(pl.multiple_of(fs * R, R), R)
+    g_ref[own, :] = (gw_ref[...] * gain).astype(jnp.bfloat16)
+    u_ref[own, :] = (uw_ref[...] * gain).astype(jnp.bfloat16)
+
+    pl.semaphore_wait(barrier, TP + jnp.where(z > 0, 1, 0) + jnp.where(z < Z - 1, 1, 0))
+
+    def piece(w, zz, yy, h):
+        return weights[w].at[pl.ds(pl.multiple_of((zz * 2 + yy) * R + h * half, half), half), :]
+
+    def move(w, zz, yy, h, sem, target):
+        ref = piece(w, zz, yy, h)
+        return pltpu.make_async_remote_copy(
+            src_ref=ref, dst_ref=ref, send_sem=sem, recv_sem=w_recv.at[w, zz * 2 + yy, h],
+            device_id=target, device_id_type=MESH,
+        )
+
+    def arrive(w, zz, yy, h):
+        move(w, zz, yy, h, hp_sem.at[w], dev(z, oy)).wait_recv()
+
+    def down_z(w, k, h, act):
+        @pl.when(jnp.logical_and(z > 0, z + k < Z))
+        def _():
+            act(move(w, z + k, y, h, zm_sem.at[w, k, h], dev(z - 1, y)))
+
+    def up_z(w, k, h, act):
+        @pl.when(jnp.logical_and(z < Z - 1, z - k >= 0))
+        def _():
+            act(move(w, z - k, y, h, zp_sem.at[w, k, h], dev(z + 1, y)))
+
+    def across(w, zz, h, act):
+        @pl.when(jnp.logical_and(zz >= 0, zz < Z))
+        def _():
+            @pl.when(jnp.logical_or(zz != pz, h != 1))
+            def _():
+                act(move(w, zz, y, h, y_sem.at[w, zz, h], dev(z, oy)))
+
+    def begin(copy):
+        copy.start()
+
+    def finish(copy):
+        copy.wait_send()
+
+    def send_own(w):
+        for h in range(2):
+            down_z(w, 0, h, begin)
+            up_z(w, 0, h, begin)
+            across(w, z, h, begin)
+
+    def event(w, e):
+        d, h = 1 + e // 2, lax.rem(e, 2)
+        for sign in (1, -1):
+            zz = z + sign * d
+
+            @pl.when(jnp.logical_and(zz >= 0, zz < Z))
+            def _():
+                arrive(w, zz, y, h)
+                (down_z if sign == 1 else up_z)(w, d, h, begin)
+                across(w, zz, h, begin)
+
+    def events(w, low, high):
+        lax.fori_loop(low, high, lambda e, c: (event(w, e), c)[1], 0)
+
+    def side(w):
+        return move(w, z, oy, 1, hp_sem.at[w], dev(pz, y))
+
+    def send_side(w):
+        arrive(w, z, oy, 1)
+        side(w).start()
+
+    def arrive_other(w, zz):
+        arrive(w, zz, oy, 0)
+
+        @pl.when(zz != z)
+        def _():
+            arrive(w, zz, oy, 1)
+
+    def arrive_rest(w):
+        lax.fori_loop(0, Z, lambda zz, c: (arrive_other(w, zz), c)[1], 0)
+
+    last = 2 * (Z - 1)
+    send_own(0)
+    send_own(1)
+
+    wide = tok_ref[...].astype(jnp.float32)
+    x_buf[pl.ds(pl.multiple_of(tp * T, T), T), :] = (
+        wide * lax.rsqrt(jnp.mean(wide * wide, axis=1, keepdims=True) + 1e-06)
+    ).astype(jnp.bfloat16)
+    d_ref[own, :] = dw_ref[...].astype(jnp.bfloat16)
+
+    def rows_to(p, owner):
+        ref = x_buf.at[pl.ds(pl.multiple_of(owner * T, T), T), :]
+        return pltpu.make_async_remote_copy(
+            src_ref=ref, dst_ref=ref, send_sem=x_send.at[p - 1], recv_sem=x_recv.at[p - 1],
+            device_id=(fs, peer(p)), device_id_type=MESH,
+        )
+
+    for p in range(1, TP):
+        rows_to(p, tp).start()
+
+    events(0, 0, 2)
+    send_own(2)
+    events(0, 2, last)
+    send_side(0)
+
+    events(1, 0, 2)
+    arrive_rest(0)
+    for p in range(1, TP):
+        rows_to(p, lax.rem(tp + TP - p, TP)).wait_recv()
+
+    wide_tile = 256
+    whole, rest = F // wide_tile, F % wide_tile
+
+    def tiles(body):
+        def step(i, c):
+            body(pl.ds(pl.multiple_of(i * wide_tile, wide_tile), wide_tile))
+            return c
+
+        lax.fori_loop(0, whole, step, 0)
+        if rest:
+            body(pl.ds(whole * wide_tile, rest))
+
+    def gate_tile(cols):
+        v = jnp.dot(x_buf[...], g_ref[:, cols], preferred_element_type=jnp.float32)
+        sg_buf[:, cols] = v / (1.0 + jnp.exp(-v))
+
+    def up_tile(cols):
+        v = jnp.dot(x_buf[...], u_ref[:, cols], preferred_element_type=jnp.float32)
+        h_buf[:, cols] = (sg_buf[:, cols] * v).astype(jnp.bfloat16)
+
+    tiles(gate_tile)
+    events(1, 2, last)
+    send_side(1)
+
+    events(2, 0, 2)
+    arrive_rest(1)
+    tiles(up_tile)
+
+    def share(p, s):
+        cols = pl.ds(pl.multiple_of(s * R, R), R)
+        return pltpu.make_async_remote_copy(
+            src_ref=part_buf.at[pl.ds(pl.multiple_of(peer(p) * T, T), T), cols],
+            dst_ref=in_buf.at[p - 1, :, cols],
+            send_sem=r_send.at[p - 1, s], recv_sem=r_recv.at[p - 1, s],
+            device_id=(fs, peer(p)), device_id_type=MESH,
+        )
+
+    def unit(zz, yy):
+        s = zz * 2 + yy
+        span = pl.ds(pl.multiple_of(s * R, R), R)
+        part_buf[:, span] = lax.dot_general(
+            h_buf[...], d_ref[span, :], (((1,), (1,)), ((), ())), preferred_element_type=jnp.float32
+        ).astype(jnp.bfloat16)
+        for p in range(1, TP):
+            share(p, s).start()
+
+    mirrored = z >= Z // 2
+    near_end = jnp.where(mirrored, Z - 1 - z, z)
+
+    def place(i):
+        at = jnp.where(i <= near_end, near_end - i, i)
+        return jnp.where(mirrored, Z - 1 - at, at)
+
+    def own_row(e, c):
+        event(2, e)
+
+        @pl.when(e == last - 1)
+        def _():
+            send_side(2)
+
+        unit(place(e - 2), y)
+        return c
+
+    lax.fori_loop(2, last, own_row, 0)
+
+    def other_row(i, c):
+        zz = place(lax.rem(i * 2, Z) + (i * 2) // Z)
+        arrive_other(2, zz)
+        unit(zz, oy)
+        return c
+
+    lax.fori_loop(0, Z, other_row, 0)
+
+    def total(q, c):
+        i = q - Z
+        s = jnp.where(
+            q < Z, place(lax.rem(q, Z)) * 2 + y, place(lax.rem(q * 2, Z) + (i * 2) // Z) * 2 + oy
+        )
+        cols = pl.ds(pl.multiple_of(s * R, R), R)
+        value = part_buf[pl.ds(pl.multiple_of(tp * T, T), T), cols].astype(jnp.float32)
+        for p in range(1, TP):
+            share(p, s).wait_recv()
+            value = value + in_buf[p - 1, :, cols].astype(jnp.float32)
+        mix_ref[:, cols] = value.astype(jnp.bfloat16)
+        for p in range(1, TP):
+            share(p, s).wait_send()
+        return c
+
+    lax.fori_loop(0, 2 * Z, total, 0)
+
+    for p in range(1, TP):
+        rows_to(p, tp).wait_send()
+    for w in range(3):
+        side(w).wait_send()
+
+        def drain(q, c):
+            k, h = q // 2, lax.rem(q, 2)
+            down_z(w, k, h, finish)
+            up_z(w, k, h, finish)
+            across(w, k, h, finish)
+            return c
+
+        lax.fori_loop(0, 2 * Z, drain, 0)
+
+
+def fused(Z, TP, tokens, norm_gain, gate_weight, up_weight, down_weight):
+    T, D = tokens.shape
+    R, F = gate_weight.shape
+    S = 2 * Z
+    whole = jax.ShapeDtypeStruct((R * S, F), jnp.bfloat16)
+    vmem = pl.BlockSpec(memory_space=pltpu.VMEM)
+    dma = pltpu.SemaphoreType.DMA
+    return pl.pallas_call(
+        functools.partial(kernel, Z, TP),
+        out_shape=(jax.ShapeDtypeStruct((T, D), jnp.bfloat16), whole, whole, whole),
+        in_specs=[vmem] * 5,
+        out_specs=(vmem,) * 4,
+        scratch_shapes=[
+            pltpu.VMEM((T * TP, D), jnp.bfloat16),
+            pltpu.VMEM((T * TP, F), jnp.float32),
+            pltpu.VMEM((T * TP, F), jnp.bfloat16),
+            pltpu.VMEM((T * TP, D), jnp.bfloat16),
+            pltpu.VMEM((TP - 1, T, D), jnp.bfloat16),
+            dma((3, Z, 2)),
+            dma((3, Z, 2)),
+            dma((3, Z, 2)),
+            dma((3,)),
+            dma((3, S, 2)),
+            dma((TP - 1,)),
+            dma((TP - 1,)),
+            dma((TP - 1, S)),
+            dma((TP - 1, S)),
+        ],
+        compiler_params=pltpu.CompilerParams(
+            collective_id=0, has_side_effects=True, vmem_limit_bytes=60 * 1024 * 1024
+        ),
+    )(tokens, norm_gain[:, None], gate_weight, up_weight, down_weight)
+
+
 def solution(mesh):
     in_specs = (P(("fs", "tp"), None), P("fs"), P("fs", "tp"), P("fs", "tp"), P("fs", "tp"))
     out_specs = (P(("fs", "tp"), None), P(None, "tp"), P(None, "tp"), P(None, "tp"))
-    return jax.shard_map(shards, mesh=mesh, in_specs=in_specs, out_specs=out_specs, check_vma=False)
+    Z, TP = mesh.shape["fs"] // 2, mesh.shape["tp"]
+
+    def step(tokens, norm_gain, gate_weight, up_weight, down_weight):
+        args = (tokens, norm_gain, gate_weight, up_weight, down_weight)
+        if mesh.shape["fs"] == 2 * TP == 8 and gate_weight.shape[1] % 128 == 0:
+            return fused(Z, TP, *args)
+        return shards(*args)
+
+    return jax.shard_map(step, mesh=mesh, in_specs=in_specs, out_specs=out_specs, check_vma=False)

time: 398 us -> 208 us (0.52)
  waiting for transfers between devices: 335 us -> 0 us
  Pallas kernels: 0 us -> 192 us
  matrix products: 27 us -> 0 us
  between operations: 13.8 us -> 0.65 us
  other arithmetic: 7.8 us -> 0.01 us
    all_gather x4 -> x0, waiting for transfers between devices: 298 us -> none  [the longest x1 95.1 us: shards(): gate_piece = lax.all_gather(gate_local, 'fs', axis=0, tiled=True)]
    pallas_call x0 -> x1, Pallas kernels: none -> 192 us  [fused(): pl.pallas_call(functools.partial(kernel, Z, TP), out_shape=(jax.ShapeDtyp...]
    reduce_scatter x1 -> x0, waiting for transfers between devices: 36.2 us -> none  [shards(): lax.psum_scatter(lax.optimization_barrier(partial_value.astype(jnp.bfloat...]
    dot_general x2 -> x0, matrix products: 27 us -> none  [the longest x1 17.3 us: shards(): lax.dot_general(hidden, down_whole, (((1,), (1,)), ((), ())), preferred_e...]
    convert_element_type x3 -> x0, other arithmetic: 6.32 us -> none  [the longest x1 3.17 us: shards(): up_local = (up_weight * row_gain).astype(jnp.bfloat16)]
    unnamed x11 -> x10, local copies, waits for them, and re-layouts: 14 us -> 13.2 us
  transfers between devices with their start and end apart: 5 -> 0, of which waited for: 5 -> 0; matrix products, arithmetic and copies ran while one was open for 3% -> 0% of each run, Pallas kernels for 0% -> 0%
where the time goes in v1:
time: 208 us
  Pallas kernels  192 us (92%)
  local copies, waits for them, and re-layouts  14.6 us (7%)
    pallas_call x1, Pallas kernels, fused(): pl.pallas_call(functools.partial(kernel, Z, TP), out_shape=(jax.ShapeDtyp...  192 us
    unnamed x10, local copies, waits for them, and re-layouts  13.2 us

profile of v1, /device:TPU:0, one launch (start us, length us, event | category | flops | bytes accessed | tf_op | source)
XLA Modules:
  0.0 207.8 jit_solution(13274341073955323811)
XLA Ops:
  0.6 1.5 copy.9.gain_ref
  2.1 192.5 %shard_map.84 = (bf16[192,2048]{1,0:T(8,128)(2,1)}, bf16[2048,1408]{1,0:T(8,128)(2,1)}, bf16[2048,1408]{1,0:T(8,128)(2,1)}, bf16[2048,1408]{1,0:T(8,128)(2,1)}) custom-call(bf16[192,2048]{1,0:T(8,128)(2,1)} %tok_ref.1, f32[256,1]{1,0:T(8,128)} %copy.9.gain_ref, f32[256,1408]{1,0:T(8,128)} %gw_ref.1, f32[256,1408]{1,0:T(8,128)} %uw_ref.1, f32[256,1408]{1,0:T(8,128)} %dw_ref.1), custom_call_target="tpu_custom_call" | custom-call | tf_op jit(solution)/shard_map/pallas_call | solution.py:306
  194.6 0.0 slice-start
  194.6 2.2 %copy.14 = bf16[192,2048]{1,0:T(8,128)(2,1)} copy(bf16[192,2048]{1,0:T(8,128)(2,1)} %get-tuple-element.8) | data formatting | bytes 1572864
  196.9 0.0 copy-start
  196.9 0.0 slice-start.1
  196.9 5.9 %copy.15 = bf16[2048,1408]{1,0:T(8,128)(2,1)} copy(bf16[2048,1408]{1,0:T(8,128)(2,1)} %get-tuple-element.9) | data formatting | bytes 11534336
  202.7 0.0 copy-done
  202.7 2.5 %copy.16 = bf16[2048,1408]{1,0:T(8,128)(2,1)} copy(bf16[2048,1408]{1,0:T(8,128)(2,1)S(1)} %copy-done) | data formatting | bytes 11534336
  205.3 0.0 slice-done
  205.3 0.0 slice-done.1
  205.3 2.5 %copy.17 = bf16[2048,1408]{1,0:T(8,128)(2,1)} copy(bf16[2048,1408]{1,0:T(8,128)(2,1)S(1)} %bitcast.2) | data formatting | bytes 11534336
  (1 shorter events, 0.0 us)
Async XLA Ops:
  194.6 10.7 %slice-start = ((s8[5767168]{0:T(1024)(128)(4,1)}), s8[4194304]{0:T(1024)(128)(4,1)S(1)}, s32[]{:S(2)}) async-start(s8[5767168]{0:T(1024)(128)(4,1)} %bitcast.1), calls=%async_computation | async-start | bytes 8388608
  196.9 5.9 %copy-start = (bf16[2048,1408]{1,0:T(8,128)(2,1)S(1)}, bf16[2048,1408]{1,0:T(8,128)(2,1)}, u32[]{:S(2)}) copy-start(bf16[2048,1408]{1,0:T(8,128)(2,1)} %get-tuple-element.10) | copy-start | bytes 17301508
  196.9 8.4 %slice-start.1 = ((s8[5767168]{0:T(1024)(128)(4,1)}), s8[1572864]{0:T(1024)(128)(4,1)S(1)}, s32[]{:S(2)}) async-start(s8[5767168]{0:T(1024)(128)(4,1)} %bitcast.1), calls=%async_computation.1 | async-start | bytes 3145728

commit v2 on v1

--- a/solution.py
+++ b/solution.py
@@ -8,6 +8,7 @@
 from jax.sharding import PartitionSpec as P
 
 MESH = pl.DeviceIdType.MESH
+N = 2
 
 
 def normalize(source):
@@ -54,7 +55,7 @@
     oy = 1 - y
     pz = z + 1 - 2 * lax.rem(z, 2)
     R, F = gw_ref.shape
-    half = R // 2
+    half = R // N
     T = tok_ref.shape[0]
     weights = (g_ref, u_ref, d_ref)
 
@@ -81,7 +82,7 @@
     def _():
         greet(dev(z + 1, y))
 
-    gain = gain_ref[...]
+    gain = jnp.broadcast_to(gain_ref[...], (128, R)).T[:, :1]
     own = pl.ds(pl.multiple_of(fs * R, R), R)
     g_ref[own, :] = (gw_ref[...] * gain).astype(jnp.bfloat16)
     u_ref[own, :] = (uw_ref[...] * gain).astype(jnp.bfloat16)
@@ -99,7 +100,7 @@
         )
 
     def arrive(w, zz, yy, h):
-        move(w, zz, yy, h, hp_sem.at[w], dev(z, oy)).wait_recv()
+        move(w, zz, yy, h, hp_sem.at[w, 0], dev(z, oy)).wait_recv()
 
     def down_z(w, k, h, act):
         @pl.when(jnp.logical_and(z > 0, z + k < Z))
@@ -114,7 +115,7 @@
     def across(w, zz, h, act):
         @pl.when(jnp.logical_and(zz >= 0, zz < Z))
         def _():
-            @pl.when(jnp.logical_or(zz != pz, h != 1))
+            @pl.when(jnp.logical_or(zz != pz, h < N // 2))
             def _():
                 act(move(w, zz, y, h, y_sem.at[w, zz, h], dev(z, oy)))
 
@@ -125,13 +126,13 @@
         copy.wait_send()
 
     def send_own(w):
-        for h in range(2):
+        for h in range(N):
             down_z(w, 0, h, begin)
             up_z(w, 0, h, begin)
             across(w, z, h, begin)
 
     def event(w, e):
-        d, h = 1 + e // 2, lax.rem(e, 2)
+        d, h = 1 + e // N, lax.rem(e, N)
         for sign in (1, -1):
             zz = z + sign * d
 
@@ -144,24 +145,27 @@
     def events(w, low, high):
         lax.fori_loop(low, high, lambda e, c: (event(w, e), c)[1], 0)
 
-    def side(w):
-        return move(w, z, oy, 1, hp_sem.at[w], dev(pz, y))
+    def side(w, h):
+        return move(w, z, oy, h, hp_sem.at[w, h - N // 2], dev(pz, y))
 
     def send_side(w):
-        arrive(w, z, oy, 1)
-        side(w).start()
+        for h in range(N // 2, N):
+            arrive(w, z, oy, h)
+            side(w, h).start()
 
     def arrive_other(w, zz):
-        arrive(w, zz, oy, 0)
+        for h in range(N // 2):
+            arrive(w, zz, oy, h)
 
         @pl.when(zz != z)
         def _():
-            arrive(w, zz, oy, 1)
+            for h in range(N // 2, N):
+                arrive(w, zz, oy, h)
 
     def arrive_rest(w):
         lax.fori_loop(0, Z, lambda zz, c: (arrive_other(w, zz), c)[1], 0)
 
-    last = 2 * (Z - 1)
+    last = N * (Z - 1)
     send_own(0)
     send_own(1)
 
@@ -181,12 +185,12 @@
     for p in range(1, TP):
         rows_to(p, tp).start()
 
-    events(0, 0, 2)
+    events(0, 0, N)
     send_own(2)
-    events(0, 2, last)
+    events(0, N, last)
     send_side(0)
 
-    events(1, 0, 2)
+    events(1, 0, N)
     arrive_rest(0)
     for p in range(1, TP):
         rows_to(p, lax.rem(tp + TP - p, TP)).wait_recv()
@@ -212,30 +216,33 @@
         h_buf[:, cols] = (sg_buf[:, cols] * v).astype(jnp.bfloat16)
 
     tiles(gate_tile)
-    events(1, 2, last)
+    events(1, N, last)
     send_side(1)
 
-    events(2, 0, 2)
+    events(2, 0, N)
     arrive_rest(1)
     tiles(up_tile)
 
-    def share(p, s):
-        cols = pl.ds(pl.multiple_of(s * R, R), R)
+    def span(zz, yy, h):
+        return pl.ds(pl.multiple_of((zz * 2 + yy) * R + h * half, half), half)
+
+    def share(p, zz, yy, h):
+        cols = span(zz, yy, h)
+        s = zz * 2 + yy
         return pltpu.make_async_remote_copy(
             src_ref=part_buf.at[pl.ds(pl.multiple_of(peer(p) * T, T), T), cols],
             dst_ref=in_buf.at[p - 1, :, cols],
-            send_sem=r_send.at[p - 1, s], recv_sem=r_recv.at[p - 1, s],
+            send_sem=r_send.at[p - 1, s, h], recv_sem=r_recv.at[p - 1, s, h],
             device_id=(fs, peer(p)), device_id_type=MESH,
         )
 
-    def unit(zz, yy):
-        s = zz * 2 + yy
-        span = pl.ds(pl.multiple_of(s * R, R), R)
-        part_buf[:, span] = lax.dot_general(
-            h_buf[...], d_ref[span, :], (((1,), (1,)), ((), ())), preferred_element_type=jnp.float32
+    def unit(zz, yy, h):
+        cols = span(zz, yy, h)
+        part_buf[:, cols] = lax.dot_general(
+            h_buf[...], d_ref[cols, :], (((1,), (1,)), ((), ())), preferred_element_type=jnp.float32
         ).astype(jnp.bfloat16)
         for p in range(1, TP):
-            share(p, s).start()
+            share(p, zz, yy, h).start()
 
     mirrored = z >= Z // 2
     near_end = jnp.where(mirrored, Z - 1 - z, z)
@@ -251,61 +258,94 @@
         def _():
             send_side(2)
 
-        unit(place(e - 2), y)
+        @pl.when(lax.rem(e, N // 2) == N // 2 - 1)
+        def _():
+            def piece_of(h, c):
+                unit(place((e - N) // (N // 2)), y, h)
+                return c
+
+            lax.fori_loop(0, N, piece_of, 0)
+
         return c
 
-    lax.fori_loop(2, last, own_row, 0)
-
-    def other_row(i, c):
-        zz = place(lax.rem(i * 2, Z) + (i * 2) // Z)
-        arrive_other(2, zz)
-        unit(zz, oy)
+    lax.fori_loop(N, last, own_row, 0)
+
+    def other(q):
+        early, pairs = q < Z * N // 2, Z // 2
+        left = q - Z * N // 2
+        i = jnp.where(early, q // N * 2, 1 + lax.rem(left + pairs * N, pairs) * 2)
+        h = jnp.where(early, lax.rem(q, N), (left + pairs * N) // pairs - N)
+        return place(i), h
+
+    def other_row(q, c):
+        zz, h = other(q)
+
+        @pl.when(jnp.logical_or(zz != z, h < N // 2))
+        def _():
+            arrive(2, zz, oy, h)
+
+        unit(zz, oy, h)
         return c
 
-    lax.fori_loop(0, Z, other_row, 0)
-
-    def total(q, c):
-        i = q - Z
-        s = jnp.where(
-            q < Z, place(lax.rem(q, Z)) * 2 + y, place(lax.rem(q * 2, Z) + (i * 2) // Z) * 2 + oy
-        )
-        cols = pl.ds(pl.multiple_of(s * R, R), R)
+    lax.fori_loop(0, Z * N, other_row, 0)
+
+    def total(zz, yy, h):
+        cols = span(zz, yy, h)
         value = part_buf[pl.ds(pl.multiple_of(tp * T, T), T), cols].astype(jnp.float32)
         for p in range(1, TP):
-            share(p, s).wait_recv()
+            share(p, zz, yy, h).wait_recv()
             value = value + in_buf[p - 1, :, cols].astype(jnp.float32)
         mix_ref[:, cols] = value.astype(jnp.bfloat16)
         for p in range(1, TP):
-            share(p, s).wait_send()
+            share(p, zz, yy, h).wait_send()
+
+    def total_own(q, c):
+        total(place(q // N), y, lax.rem(q, N))
         return c
 
-    lax.fori_loop(0, 2 * Z, total, 0)
+    def total_other(q, c):
+        zz, h = other(q)
+        total(zz, oy, h)
+        return c
+
+    lax.fori_loop(0, Z * N, total_own, 0)
+    lax.fori_loop(0, Z * N, total_other, 0)
 
     for p in range(1, TP):
         rows_to(p, tp).wait_send()
     for w in range(3):
-        side(w).wait_send()
+        for h in range(N // 2, N):
+            side(w, h).wait_send()
 
         def drain(q, c):
-            k, h = q // 2, lax.rem(q, 2)
+            k, h = q // N, lax.rem(q, N)
             down_z(w, k, h, finish)
             up_z(w, k, h, finish)
             across(w, k, h, finish)
             return c
 
-        lax.fori_loop(0, 2 * Z, drain, 0)
+        lax.fori_loop(0, N * Z, drain, 0)
+
+
+def store(*refs):
+    sems = refs[8]
+    copies = [pltpu.make_async_copy(refs[i], refs[4 + i], sems.at[i]) for i in range(4)]
+    for copy in copies:
+        copy.start()
+    for copy in copies:
+        copy.wait()
 
 
 def fused(Z, TP, tokens, norm_gain, gate_weight, up_weight, down_weight):
     T, D = tokens.shape
     R, F = gate_weight.shape
     S = 2 * Z
-    whole = jax.ShapeDtypeStruct((R * S, F), jnp.bfloat16)
+    whole = pltpu.VMEM((R * S, F), jnp.bfloat16)
     vmem = pl.BlockSpec(memory_space=pltpu.VMEM)
     dma = pltpu.SemaphoreType.DMA
-    return pl.pallas_call(
+    results = pl.pallas_call(
         functools.partial(kernel, Z, TP),
-        out_shape=(jax.ShapeDtypeStruct((T, D), jnp.bfloat16), whole, whole, whole),
+        out_shape=(pltpu.VMEM((T, D), jnp.bfloat16), whole, whole, whole),
         in_specs=[vmem] * 5,
         out_specs=(vmem,) * 4,
         scratch_shapes=[
@@ -314,20 +354,28 @@
             pltpu.VMEM((T * TP, F), jnp.bfloat16),
             pltpu.VMEM((T * TP, D), jnp.bfloat16),
             pltpu.VMEM((TP - 1, T, D), jnp.bfloat16),
-            dma((3, Z, 2)),
-            dma((3, Z, 2)),
-            dma((3, Z, 2)),
-            dma((3,)),
-            dma((3, S, 2)),
+            dma((3, Z, N)),
+            dma((3, Z, N)),
+            dma((3, Z, N)),
+            dma((3, N // 2)),
+            dma((3, S, N)),
             dma((TP - 1,)),
             dma((TP - 1,)),
-            dma((TP - 1, S)),
-            dma((TP - 1, S)),
+            dma((TP - 1, S, N)),
+            dma((TP - 1, S, N)),
         ],
         compiler_params=pltpu.CompilerParams(
-            collective_id=0, has_side_effects=True, vmem_limit_bytes=60 * 1024 * 1024
+            collective_id=0, has_side_effects=True, vmem_limit_bytes=36 * 1024 * 1024
         ),
-    )(tokens, norm_gain[:, None], gate_weight, up_weight, down_weight)
+    )(tokens, norm_gain[None, :], gate_weight, up_weight, down_weight)
+    return pl.pallas_call(
+        store,
+        out_shape=[jax.ShapeDtypeStruct(r.shape, r.dtype) for r in results],
+        in_specs=[vmem] * 4,
+        out_specs=[pl.BlockSpec(memory_space=pl.ANY)] * 4,
+        scratch_shapes=[dma((4,))],
+        compiler_params=pltpu.CompilerParams(vmem_limit_bytes=1024 * 1024),
+    )(*results)
 
 
 def solution(mesh):

time: 208 us -> 195 us (0.938)
  local copies, waits for them, and re-layouts: 14.6 us -> 0.67 us
    unnamed x10 -> x2, local copies, waits for them, and re-layouts: 13.2 us -> 0.67 us
    pallas_call x1 -> x2, Pallas kernels: 192 us -> 194 us  [the longest x1 187 us: fused(): pl.pallas_call(functools.partial(kernel, Z, TP), out_shape=(pltpu.VMEM((T...]
where the time goes in v2:
time: 195 us
  Pallas kernels  194 us (99%)
    pallas_call x1, Pallas kernels, fused(): pl.pallas_call(functools.partial(kernel, Z, TP), out_shape=(pltpu.VMEM((T...  187 us
    pallas_call x1, Pallas kernels, fused(): pl.pallas_call(store, out_shape=[jax.ShapeDtypeStruct(r.shape, r.dtype) f...  6.46 us

profile of v2, /device:TPU:0, one launch (start us, length us, event | category | flops | bytes accessed | tf_op | source)
XLA Modules:
  0.0 194.9 jit_solution(7705437901328317182)
XLA Ops:
  0.6 0.0 copy-start
  0.6 0.7 copy-done
  1.3 187.1 %shard_map.84 = (bf16[192,2048]{1,0:T(8,128)(2,1)S(1)}, bf16[2048,1408]{1,0:T(8,128)(2,1)S(1)}, bf16[2048,1408]{1,0:T(8,128)(2,1)S(1)}, bf16[2048,1408]{1,0:T(8,128)(2,1)S(1)}) custom-call(bf16[192,2048]{1,0:T(8,128)(2,1)} %tok_ref.1, f32[1,256]{1,0:T(1,128)S(1)} %bitcast.1, f32[256,1408]{1,0:T(8,128)} %gw_ref.1, f32[256,1408]{1,0:T(8,128)} %uw_ref.1, ...), custom_call_target="tpu_custom_call" | custom-call | tf_op jit(solution)/shard_map/pallas_call | solution.py:346
  188.4 6.5 %shard_map.85 = (bf16[192,2048]{1,0:T(8,128)(2,1)}, bf16[2048,1408]{1,0:T(8,128)(2,1)}, bf16[2048,1408]{1,0:T(8,128)(2,1)}, bf16[2048,1408]{1,0:T(8,128)(2,1)}) custom-call(bf16[192,2048]{1,0:T(8,128)(2,1)S(1)} %get-tuple-element.8.refs_0_, bf16[2048,1408]{1,0:T(8,128)(2,1)S(1)} %get-tuple-element.9.refs_1_, ...), custom_call_target="tpu_custom_call" | custom-call | tf_op jit(solution)/shard_map/pallas_call | solution.py:371
Async XLA Ops:
  0.6 0.7 copy-start
